TPU v7x, 128 devices: a whole 4x4x4 slice. The times are simulated.
128 devices in a mesh: sp: 16 (over z, x), tp: 8 (over y, core).
Axes of the slice: x: 4, y: 4, z: 4, core: 2. Of those that a mesh axis runs over, the one named last changes fastest.
Arguments:
- queries: bfloat16 [16384, 512], P('sp', 'tp'), may hold values from -9.5625 to 9.5625
- keys: bfloat16 [16384, 512], P('sp', 'tp'), may hold values from -9.5625 to 9.5625
- values: bfloat16 [16384, 512], P('sp', 'tp'), may hold values from -6 to 6
- key_bias: bfloat16 [16384, 8], P('sp', 'tp'), may hold values from -17 to 0
- residual: bfloat16 [16384, 2048], P(('sp', 'tp')), may hold values from -6 to 6
- out_weight: bfloat16 [512, 2048], replicated, may hold values from -1 to 1
- norm_gain: float32 [2048], replicated, may hold values from 0.1 to 1.9
- routes: int32 [16384, 2], P(('sp', 'tp')), may hold values from 0 to 15, all different within a row; in each aligned block of 128 rows (0 to 127, 128 to 255, ...) at most 20 rows name the same one
- route_weights: float32 [16384, 2], P(('sp', 'tp')), may hold values from 0.25 to 2
- gate_weight: bfloat16 [16, 2048, 4096], P('sp', None, 'tp'), may hold values from -0.125 to 0.125
- up_weight: bfloat16 [16, 2048, 4096], P('sp', None, 'tp'), may hold values from -0.125 to 0.125
- down_weight: bfloat16 [16, 4096, 2048], P('sp', 'tp'), may hold values from -0.09375 to 0.09375
Outputs:
- output: bfloat16 [16384, 2048], P(('sp', 'tp'))
Inputs may be any that keep to these rules, and one draw needn't show every extreme that they name: `routes`: each row names 2 different experts; the rows of one device name no expert more than 20 times.
All inputs are finite; a program needn't handle non-finite values.
Results may differ from a plain program's by a relative error of at most 0.017.
Values may be sent and summed in bfloat16 or wider, within the bound.
A program may use at most 128 MiB of HBM per device.

v0:
```python
import jax
import jax.numpy as jnp
from jax import lax
from jax.sharding import PartitionSpec as P

HEAD_DIM = 64
TOP = 2
SPAN = 512


epsilon = 1e-06


def sent_together(arrays, axis, dim, along):
    ends, at = ([], 0)
    for a in arrays[:-1]:
        at += a.shape[along]
        ends.append(at)
    both = jnp.concatenate(arrays, axis=along)
    return tuple(jnp.split(lax.all_gather(both, axis, axis=dim, tiled=True), ends, axis=along))


def joined_along(blocks, dim):
    blocks = jnp.moveaxis(blocks, 0, dim)
    shape = blocks.shape
    return blocks.reshape(*shape[:dim], shape[dim] * shape[dim + 1], *shape[dim + 2 :])


def on_gathered_pieces(array, axis, dim, apply, out_dim):
    size, width = (lax.axis_size(axis), array.shape[dim])
    count = 2 if width % 2 == 0 else 1
    finished, length = ([], width // count)
    for k in range(count):
        section = lax.slice_in_dim(array, k * length, (k + 1) * length, axis=dim)
        starts = jnp.arange(size) * width + k * length
        finished.append(jax.vmap(apply)(lax.all_gather(section, axis), starts))
    return joined_along(jnp.concatenate(finished, axis=out_dim + 1), out_dim)


def shards(
    queries,
    keys,
    values,
    key_bias,
    residual,
    out_weight,
    norm_gain,
    routes,
    route_weights,
    gate_weight,
    up_weight,
    down_weight,
):
    shard_len = queries.shape[0]
    local_heads = key_bias.shape[1]
    sp_count = lax.axis_size("sp")
    offset = lax.axis_index("sp") * shard_len
    query_heads = queries.reshape(shard_len, local_heads, HEAD_DIM)
    query_pos = offset + lax.iota(jnp.int32, shard_len)
    score_scale = HEAD_DIM ** (-0.5)
    slot_count = sp_count * shard_len // SPAN

    def span_terms(key_rows, value_rows, bias_rows, key_first):
        scores = jnp.einsum(
            "qhd,khd->qhk",
            query_heads,
            key_rows.reshape(SPAN, local_heads, HEAD_DIM),
            preferred_element_type=jnp.float32,
        )
        scores = scores * score_scale + jnp.transpose(bias_rows.astype(jnp.float32))[None, :, :]
        key_pos = key_first + lax.iota(jnp.int32, SPAN)
        earlier = key_pos[None, None, :] < query_pos[:, None, None]
        failure = jnp.where(earlier, jax.nn.log_sigmoid(-scores), 0.0)
        later_sum = lax.cumsum(failure, axis=2, reverse=True) - failure
        weights = jnp.where(earlier, jnp.exp(jax.nn.log_sigmoid(scores) + later_sum), 0.0).astype(
            jnp.bfloat16
        )
        span_out = jnp.einsum(
            "qhk,khd->qhd",
            weights,
            value_rows.reshape(SPAN, local_heads, HEAD_DIM),
            preferred_element_type=jnp.float32,
        )
        return (span_out, jnp.sum(failure, axis=2))

    def skipped():
        return (
            jnp.zeros((shard_len, local_heads, HEAD_DIM), jnp.float32),
            jnp.zeros((shard_len, local_heads), jnp.float32),
        )

    empty_pair = (
        jnp.zeros((slot_count, shard_len, local_heads, HEAD_DIM), jnp.float32),
        jnp.zeros((slot_count, shard_len, local_heads), jnp.float32),
    )
    key_piece, value_piece, bias_piece = sent_together((keys, values, key_bias), "sp", 0, 1)
    span_total = key_piece.shape[0] // SPAN

    def place_span(which, held):
        outs_held, totals_held = held
        row_begin = which * SPAN

        def compute():
            return span_terms(
                lax.dynamic_slice_in_dim(key_piece, row_begin, SPAN, 0),
                lax.dynamic_slice_in_dim(value_piece, row_begin, SPAN, 0),
                lax.dynamic_slice_in_dim(bias_piece, row_begin, SPAN, 0),
                row_begin,
            )

        span_out, span_sum = lax.cond(row_begin < offset + shard_len, compute, skipped)
        slot = row_begin // SPAN
        return (
            lax.dynamic_update_index_in_dim(outs_held, span_out, slot, 0),
            lax.dynamic_update_index_in_dim(totals_held, span_sum, slot, 0),
        )

    span_outs, span_sums = lax.fori_loop(0, span_total, place_span, empty_pair)
    after_span = lax.cumsum(span_sums, axis=0, reverse=True) - span_sums
    attended = jnp.sum(jnp.exp(after_span)[..., None] * span_outs, axis=0)
    attended = attended.reshape(shard_len, local_heads * HEAD_DIM).astype(jnp.bfloat16)
    token_heads = lax.all_to_all(attended, "tp", split_axis=0, concat_axis=1, tiled=True)
    projected = jnp.dot(token_heads, out_weight, preferred_element_type=jnp.float32)
    stream = (residual.astype(jnp.float32) + projected).astype(jnp.bfloat16).astype(jnp.float32)
    normed = (
        stream * lax.rsqrt(jnp.mean(stream * stream, axis=-1, keepdims=True) + epsilon) * norm_gain
    ).astype(jnp.bfloat16)
    token_count = residual.shape[0]
    width_model = residual.shape[1]
    capacity = max(2, 5 * token_count * TOP // (4 * sp_count))
    flat_routes = routes.reshape(-1)
    onehot = (flat_routes[:, None] == lax.iota(jnp.int32, sp_count)[None, :]).astype(jnp.int32)
    before = jnp.cumsum(onehot, axis=0) - onehot
    slot_of = flat_routes * capacity + jnp.sum(before * onehot, axis=1)
    select = (slot_of[:, None] == lax.iota(jnp.int32, sp_count * capacity)[None, :]).astype(
        jnp.bfloat16
    )
    placing = jnp.sum(select.reshape(token_count, TOP, sp_count * capacity), axis=1)
    outgoing = jnp.einsum("ts,td->sd", placing, normed, preferred_element_type=jnp.float32).astype(
        jnp.bfloat16
    )
    arrived = lax.all_to_all(outgoing, "sp", split_axis=0, concat_axis=0, tiled=True)

    def fan_hidden(row_block, first_row):
        gate_act = jnp.dot(row_block, gate_weight[0], preferred_element_type=jnp.float32)
        up_act = jnp.dot(row_block, up_weight[0], preferred_element_type=jnp.float32)
        return (jax.nn.silu(gate_act) * up_act).astype(jnp.bfloat16)

    hidden = on_gathered_pieces(arrived, "tp", 0, fan_hidden, 0)
    partial_value = jnp.dot(hidden, down_weight[0], preferred_element_type=jnp.float32)
    summed = lax.psum_scatter(
        lax.optimization_barrier(partial_value.astype(jnp.bfloat16))
        .astype(jnp.float32)
        .astype(jnp.bfloat16),
        "tp",
        scatter_dimension=0,
        tiled=True,
    )
    returned = lax.all_to_all(summed, "sp", split_axis=0, concat_axis=0, tiled=True)
    picked = jnp.dot(select, returned, preferred_element_type=jnp.float32).reshape(
        token_count, TOP, width_model
    )
    routed = jnp.sum(picked * route_weights[:, :, None], axis=1)
    return (stream + routed).astype(jnp.bfloat16)


def solution(mesh):
    return jax.shard_map(
        shards,
        mesh=mesh,
        in_specs=(
            P("sp", "tp"),
            P("sp", "tp"),
            P("sp", "tp"),
            P("sp", "tp"),
            P(("sp", "tp"), None),
            P(),
            P(),
            P(("sp", "tp"), None),
            P(("sp", "tp"), None),
            P("sp", None, "tp"),
            P("sp", None, "tp"),
            P("sp", "tp", None),
        ),
        out_specs=P(("sp", "tp"), None),
        check_vma=False,
    )
```

profile of v0, /device:TPU:64, one launch (start us, length us, event | category | flops | bytes accessed | tf_op | source)
XLA Modules:
  0.0 1093.5 jit_solution(10400718059973786038)
XLA Ops:
  11.3 52.2 %all-gather.4.cloned.1.call-done = bf16[16384,129]{0,1:T(8,128)(2,1)} async-done(((bf16[1024,129]{0,1:T(8,128)(2,1)}), bf16[16384,129]{0,1:T(8,128)(2,1)}) %all-gather.4.cloned.1.call-update) | async-done | bytes 4227088 | tf_op jit(solution)/shard_map/all_gather | solution.py:20
  73.1 4.9 copy.68
  83.3 438.0 %while.18 = (s32[]{:T(128)}, f32[32,1024,1,64]{1,3,2,0:T(8,128)}, f32[32,1024,1]{1,2,0:T(1,128)S(1)}, s32[]{:T(128)}, bf16[16384,64]{1,0:T(8,128)(2,1)}, /*index...) while((s32[]{:T(128)}, f32[32,1024,1,64]{1,3,2,0:T(8,128)}, ...), condition=%wide.region_6.7_spmd.clone, body=%wide.region_0.6_spmd.clone.sunk | while | flops 219693056 | bytes 49579584 | solution.py:118
  83.5 23.0 %conditional.3 = (f32[1,1024,1,64]{1,3,2,0:T(8,128)S(1)}, f32[1,1024,1]{1,2,0:T(1,128)S(1)}) conditional(s32[]{:T(128)} %convert_element_type.98, () %tuple.66, (s32[]{:T(128)}, bf16[16384,64]{1,0:T(8,128)(2,1)}, s32[]{:T(128)}, bf16[16384,64]{1,0:T(8,128)(2,1)}, bf16[1024,1,64]{0,2,1:T(8,128)(2,1)S(1)}, /*index=5*/bf16[16384,1]{0,1:T(2,128)(2,1)S(1)}, ...), branch_computations={%region_1.0_spmd, %region_2.5_spmd} | conditional | flops 219693056 | bytes 49042592 | solution.py:111
  87.5 9.6 fusion.12
  107.3 23.0 %conditional.3 = (f32[1,1024,1,64]{1,3,2,0:T(8,128)S(1)}, f32[1,1024,1]{1,2,0:T(1,128)S(1)}) conditional(s32[]{:T(128)} %convert_element_type.98, () %tuple.66, (s32[]{:T(128)}, bf16[16384,64]{1,0:T(8,128)(2,1)}, s32[]{:T(128)}, bf16[16384,64]{1,0:T(8,128)(2,1)}, bf16[1024,1,64]{0,2,1:T(8,128)(2,1)S(1)}, /*index=5*/bf16[16384,1]{0,1:T(2,128)(2,1)S(1)}, ...), branch_computations={%region_1.0_spmd, %region_2.5_spmd} | conditional | flops 219693056 | bytes 49042592 | solution.py:111
  111.2 9.6 fusion.12
  131.0 23.0 %conditional.3 = (f32[1,1024,1,64]{1,3,2,0:T(8,128)S(1)}, f32[1,1024,1]{1,2,0:T(1,128)S(1)}) conditional(s32[]{:T(128)} %convert_element_type.98, () %tuple.66, (s32[]{:T(128)}, bf16[16384,64]{1,0:T(8,128)(2,1)}, s32[]{:T(128)}, bf16[16384,64]{1,0:T(8,128)(2,1)}, bf16[1024,1,64]{0,2,1:T(8,128)(2,1)S(1)}, /*index=5*/bf16[16384,1]{0,1:T(2,128)(2,1)S(1)}, ...), branch_computations={%region_1.0_spmd, %region_2.5_spmd} | conditional | flops 219693056 | bytes 49042592 | solution.py:111
  134.9 9.6 fusion.12
  154.7 23.0 %conditional.3 = (f32[1,1024,1,64]{1,3,2,0:T(8,128)S(1)}, f32[1,1024,1]{1,2,0:T(1,128)S(1)}) conditional(s32[]{:T(128)} %convert_element_type.98, () %tuple.66, (s32[]{:T(128)}, bf16[16384,64]{1,0:T(8,128)(2,1)}, s32[]{:T(128)}, bf16[16384,64]{1,0:T(8,128)(2,1)}, bf16[1024,1,64]{0,2,1:T(8,128)(2,1)S(1)}, /*index=5*/bf16[16384,1]{0,1:T(2,128)(2,1)S(1)}, ...), branch_computations={%region_1.0_spmd, %region_2.5_spmd} | conditional | flops 219693056 | bytes 49042592 | solution.py:111
  158.6 9.6 fusion.12
  178.4 23.0 %conditional.3 = (f32[1,1024,1,64]{1,3,2,0:T(8,128)S(1)}, f32[1,1024,1]{1,2,0:T(1,128)S(1)}) conditional(s32[]{:T(128)} %convert_element_type.98, () %tuple.66, (s32[]{:T(128)}, bf16[16384,64]{1,0:T(8,128)(2,1)}, s32[]{:T(128)}, bf16[16384,64]{1,0:T(8,128)(2,1)}, bf16[1024,1,64]{0,2,1:T(8,128)(2,1)S(1)}, /*index=5*/bf16[16384,1]{0,1:T(2,128)(2,1)S(1)}, ...), branch_computations={%region_1.0_spmd, %region_2.5_spmd} | conditional | flops 219693056 | bytes 49042592 | solution.py:111
  182.3 9.6 fusion.12
  202.1 23.0 %conditional.3 = (f32[1,1024,1,64]{1,3,2,0:T(8,128)S(1)}, f32[1,1024,1]{1,2,0:T(1,128)S(1)}) conditional(s32[]{:T(128)} %convert_element_type.98, () %tuple.66, (s32[]{:T(128)}, bf16[16384,64]{1,0:T(8,128)(2,1)}, s32[]{:T(128)}, bf16[16384,64]{1,0:T(8,128)(2,1)}, bf16[1024,1,64]{0,2,1:T(8,128)(2,1)S(1)}, /*index=5*/bf16[16384,1]{0,1:T(2,128)(2,1)S(1)}, ...), branch_computations={%region_1.0_spmd, %region_2.5_spmd} | conditional | flops 219693056 | bytes 49042592 | solution.py:111
  206.0 9.6 fusion.12
  225.8 23.0 %conditional.3 = (f32[1,1024,1,64]{1,3,2,0:T(8,128)S(1)}, f32[1,1024,1]{1,2,0:T(1,128)S(1)}) conditional(s32[]{:T(128)} %convert_element_type.98, () %tuple.66, (s32[]{:T(128)}, bf16[16384,64]{1,0:T(8,128)(2,1)}, s32[]{:T(128)}, bf16[16384,64]{1,0:T(8,128)(2,1)}, bf16[1024,1,64]{0,2,1:T(8,128)(2,1)S(1)}, /*index=5*/bf16[16384,1]{0,1:T(2,128)(2,1)S(1)}, ...), branch_computations={%region_1.0_spmd, %region_2.5_spmd} | conditional | flops 219693056 | bytes 49042592 | solution.py:111
  229.7 9.6 fusion.12
  249.5 23.0 %conditional.3 = (f32[1,1024,1,64]{1,3,2,0:T(8,128)S(1)}, f32[1,1024,1]{1,2,0:T(1,128)S(1)}) conditional(s32[]{:T(128)} %convert_element_type.98, () %tuple.66, (s32[]{:T(128)}, bf16[16384,64]{1,0:T(8,128)(2,1)}, s32[]{:T(128)}, bf16[16384,64]{1,0:T(8,128)(2,1)}, bf16[1024,1,64]{0,2,1:T(8,128)(2,1)S(1)}, /*index=5*/bf16[16384,1]{0,1:T(2,128)(2,1)S(1)}, ...), branch_computations={%region_1.0_spmd, %region_2.5_spmd} | conditional | flops 219693056 | bytes 49042592 | solution.py:111
  253.4 9.6 fusion.12
  273.2 23.0 %conditional.3 = (f32[1,1024,1,64]{1,3,2,0:T(8,128)S(1)}, f32[1,1024,1]{1,2,0:T(1,128)S(1)}) conditional(s32[]{:T(128)} %convert_element_type.98, () %tuple.66, (s32[]{:T(128)}, bf16[16384,64]{1,0:T(8,128)(2,1)}, s32[]{:T(128)}, bf16[16384,64]{1,0:T(8,128)(2,1)}, bf16[1024,1,64]{0,2,1:T(8,128)(2,1)S(1)}, /*index=5*/bf16[16384,1]{0,1:T(2,128)(2,1)S(1)}, ...), branch_computations={%region_1.0_spmd, %region_2.5_spmd} | conditional | flops 219693056 | bytes 49042592 | solution.py:111
  277.1 9.6 fusion.12
  296.9 23.0 %conditional.3 = (f32[1,1024,1,64]{1,3,2,0:T(8,128)S(1)}, f32[1,1024,1]{1,2,0:T(1,128)S(1)}) conditional(s32[]{:T(128)} %convert_element_type.98, () %tuple.66, (s32[]{:T(128)}, bf16[16384,64]{1,0:T(8,128)(2,1)}, s32[]{:T(128)}, bf16[16384,64]{1,0:T(8,128)(2,1)}, bf16[1024,1,64]{0,2,1:T(8,128)(2,1)S(1)}, /*index=5*/bf16[16384,1]{0,1:T(2,128)(2,1)S(1)}, ...), branch_computations={%region_1.0_spmd, %region_2.5_spmd} | conditional | flops 219693056 | bytes 49042592 | solution.py:111
  300.8 9.6 fusion.12
  320.6 23.0 %conditional.3 = (f32[1,1024,1,64]{1,3,2,0:T(8,128)S(1)}, f32[1,1024,1]{1,2,0:T(1,128)S(1)}) conditional(s32[]{:T(128)} %convert_element_type.98, () %tuple.66, (s32[]{:T(128)}, bf16[16384,64]{1,0:T(8,128)(2,1)}, s32[]{:T(128)}, bf16[16384,64]{1,0:T(8,128)(2,1)}, bf16[1024,1,64]{0,2,1:T(8,128)(2,1)S(1)}, /*index=5*/bf16[16384,1]{0,1:T(2,128)(2,1)S(1)}, ...), branch_computations={%region_1.0_spmd, %region_2.5_spmd} | conditional | flops 219693056 | bytes 49042592 | solution.py:111
  324.5 9.6 fusion.12
  344.3 23.0 %conditional.3 = (f32[1,1024,1,64]{1,3,2,0:T(8,128)S(1)}, f32[1,1024,1]{1,2,0:T(1,128)S(1)}) conditional(s32[]{:T(128)} %convert_element_type.98, () %tuple.66, (s32[]{:T(128)}, bf16[16384,64]{1,0:T(8,128)(2,1)}, s32[]{:T(128)}, bf16[16384,64]{1,0:T(8,128)(2,1)}, bf16[1024,1,64]{0,2,1:T(8,128)(2,1)S(1)}, /*index=5*/bf16[16384,1]{0,1:T(2,128)(2,1)S(1)}, ...), branch_computations={%region_1.0_spmd, %region_2.5_spmd} | conditional | flops 219693056 | bytes 49042592 | solution.py:111
  348.2 9.6 fusion.12
  368.1 23.0 %conditional.3 = (f32[1,1024,1,64]{1,3,2,0:T(8,128)S(1)}, f32[1,1024,1]{1,2,0:T(1,128)S(1)}) conditional(s32[]{:T(128)} %convert_element_type.98, () %tuple.66, (s32[]{:T(128)}, bf16[16384,64]{1,0:T(8,128)(2,1)}, s32[]{:T(128)}, bf16[16384,64]{1,0:T(8,128)(2,1)}, bf16[1024,1,64]{0,2,1:T(8,128)(2,1)S(1)}, /*index=5*/bf16[16384,1]{0,1:T(2,128)(2,1)S(1)}, ...), branch_computations={%region_1.0_spmd, %region_2.5_spmd} | conditional | flops 219693056 | bytes 49042592 | solution.py:111
  371.9 9.6 fusion.12
  391.8 23.0 %conditional.3 = (f32[1,1024,1,64]{1,3,2,0:T(8,128)S(1)}, f32[1,1024,1]{1,2,0:T(1,128)S(1)}) conditional(s32[]{:T(128)} %convert_element_type.98, () %tuple.66, (s32[]{:T(128)}, bf16[16384,64]{1,0:T(8,128)(2,1)}, s32[]{:T(128)}, bf16[16384,64]{1,0:T(8,128)(2,1)}, bf16[1024,1,64]{0,2,1:T(8,128)(2,1)S(1)}, /*index=5*/bf16[16384,1]{0,1:T(2,128)(2,1)S(1)}, ...), branch_computations={%region_1.0_spmd, %region_2.5_spmd} | conditional | flops 219693056 | bytes 49042592 | solution.py:111
  395.7 9.6 fusion.12
  415.5 23.0 %conditional.3 = (f32[1,1024,1,64]{1,3,2,0:T(8,128)S(1)}, f32[1,1024,1]{1,2,0:T(1,128)S(1)}) conditional(s32[]{:T(128)} %convert_element_type.98, () %tuple.66, (s32[]{:T(128)}, bf16[16384,64]{1,0:T(8,128)(2,1)}, s32[]{:T(128)}, bf16[16384,64]{1,0:T(8,128)(2,1)}, bf16[1024,1,64]{0,2,1:T(8,128)(2,1)S(1)}, /*index=5*/bf16[16384,1]{0,1:T(2,128)(2,1)S(1)}, ...), branch_computations={%region_1.0_spmd, %region_2.5_spmd} | conditional | flops 219693056 | bytes 49042592 | solution.py:111
  419.4 9.6 fusion.12
  439.2 23.0 %conditional.3 = (f32[1,1024,1,64]{1,3,2,0:T(8,128)S(1)}, f32[1,1024,1]{1,2,0:T(1,128)S(1)}) conditional(s32[]{:T(128)} %convert_element_type.98, () %tuple.66, (s32[]{:T(128)}, bf16[16384,64]{1,0:T(8,128)(2,1)}, s32[]{:T(128)}, bf16[16384,64]{1,0:T(8,128)(2,1)}, bf16[1024,1,64]{0,2,1:T(8,128)(2,1)S(1)}, /*index=5*/bf16[16384,1]{0,1:T(2,128)(2,1)S(1)}, ...), branch_computations={%region_1.0_spmd, %region_2.5_spmd} | conditional | flops 219693056 | bytes 49042592 | solution.py:111
  443.1 9.6 fusion.12
  462.9 23.0 %conditional.3 = (f32[1,1024,1,64]{1,3,2,0:T(8,128)S(1)}, f32[1,1024,1]{1,2,0:T(1,128)S(1)}) conditional(s32[]{:T(128)} %convert_element_type.98, () %tuple.66, (s32[]{:T(128)}, bf16[16384,64]{1,0:T(8,128)(2,1)}, s32[]{:T(128)}, bf16[16384,64]{1,0:T(8,128)(2,1)}, bf16[1024,1,64]{0,2,1:T(8,128)(2,1)S(1)}, /*index=5*/bf16[16384,1]{0,1:T(2,128)(2,1)S(1)}, ...), branch_computations={%region_1.0_spmd, %region_2.5_spmd} | conditional | flops 219693056 | bytes 49042592 | solution.py:111
  466.8 9.6 fusion.12
  486.6 23.0 %conditional.3 = (f32[1,1024,1,64]{1,3,2,0:T(8,128)S(1)}, f32[1,1024,1]{1,2,0:T(1,128)S(1)}) conditional(s32[]{:T(128)} %convert_element_type.98, () %tuple.66, (s32[]{:T(128)}, bf16[16384,64]{1,0:T(8,128)(2,1)}, s32[]{:T(128)}, bf16[16384,64]{1,0:T(8,128)(2,1)}, bf16[1024,1,64]{0,2,1:T(8,128)(2,1)S(1)}, /*index=5*/bf16[16384,1]{0,1:T(2,128)(2,1)S(1)}, ...), branch_computations={%region_1.0_spmd, %region_2.5_spmd} | conditional | flops 219693056 | bytes 49042592 | solution.py:111
  490.5 9.6 fusion.12
  531.6 6.0 all-to-all-done
  544.7 345.8 %all_to_all.37 = bf16[16,20,2048]{2,1,0:T(8,128)(2,1)S(1)} all-to-all(bf16[16,20,2048]{2,1,0:T(8,128)(2,1)} %all_to_all.29), channel_id=1, replica_groups=mesh['sp'=16,'tp'=8] {'sp'}, dimensions={0} | all-to-all | bytes 2621440 | tf_op jit(solution)/shard_map/all_to_all | solution.py:142
  896.1 32.3 %all-gather.6.cloned.1.call-done = bf16[8,160,2048]{2,1,0:T(8,128)(2,1)} async-done(((bf16[1,160,2048]{2,1,0:T(8,128)(2,1)}), bf16[8,160,2048]{2,1,0:T(8,128)(2,1)}) %all-gather.6.cloned.1.call-update) | async-done | bytes 5242896 | tf_op jit(solution)/shard_map/all_gather | solution.py:36
  928.4 7.6 fusion.27
  935.9 30.6 %all-gather.8.cloned.1.call-done = bf16[8,160,2048]{2,1,0:T(8,128)(2,1)} async-done(((bf16[1,160,2048]{2,1,0:T(8,128)(2,1)}), bf16[8,160,2048]{2,1,0:T(8,128)(2,1)}) %all-gather.8.cloned.1.call-update) | async-done | bytes 5242896 | tf_op jit(solution)/shard_map/all_gather | solution.py:36
  966.6 5.6 fusion.25
  979.5 8.2 convolution_convert_fusion
  987.8 62.6 %reduce-scatter.2.cloned.1.call-done = bf16[320,2048]{1,0:T(8,128)(2,1)} async-done(((bf16[2560,2048]{1,0:T(8,128)(2,1)}), bf16[320,2048]{1,0:T(8,128)(2,1)}) %reduce-scatter.2.cloned.1.call-update) | async-done | bytes 1310736 | tf_op jit(solution)/shard_map/reduce_scatter | solution.py:151
  1053.6 27.0 %all_to_all.38 = bf16[16,20,2048]{2,1,0:T(8,128)(2,1)} all-to-all(bf16[16,20,2048]{2,1,0:T(8,128)(2,1)} %all_to_all.31), channel_id=1, replica_groups=mesh['sp'=16,'tp'=8] {'sp'}, dimensions={0} | all-to-all | bytes 2621440 | tf_op jit(solution)/shard_map/all_to_all | solution.py:159
  (509 shorter events, 322.6 us)
Async XLA Ops:
  6.5 973.0 %copy-start = (bf16[1,512,2048]{2,1,0:T(8,128)(2,1)S(1)}, bf16[1,512,2048]{2,1,0:T(8,128)(2,1)}, u32[]{:S(2)}) copy-start(bf16[1,512,2048]{2,1,0:T(8,128)(2,1)} %param.27) | copy-start | bytes 6291460
  6.5 57.1 %all-gather.4.cloned.1.call-start = ((), (), s32[]{:S(2)}) async-start(), calls=%async_computation.4 | async-start | bytes 4734976 | tf_op jit(solution)/shard_map/all_gather | solution.py:20
  78.9 4.4 copy-start.7
  98.5 1.6 copy-start.2
  100.0 1.6 copy-start.3
  122.1 1.6 copy-start.2
  123.7 1.6 copy-start.3
  145.8 1.6 copy-start.2
  147.4 1.6 copy-start.3
  169.5 1.6 copy-start.2
  171.1 1.6 copy-start.3
  193.3 1.6 copy-start.2
  194.8 1.6 copy-start.3
  217.0 1.6 copy-start.2
  218.6 1.6 copy-start.3
  240.7 1.6 copy-start.2
  242.3 1.6 copy-start.3
  264.4 1.6 copy-start.2
  266.0 1.6 copy-start.3
  288.1 1.6 copy-start.2
  289.7 1.6 copy-start.3
  311.8 1.6 copy-start.2
  313.4 1.6 copy-start.3
  335.5 1.6 copy-start.2
  337.1 1.6 copy-start.3
  359.2 1.6 copy-start.2
  360.8 1.6 copy-start.3
  382.9 1.6 copy-start.2
  406.6 1.6 copy-start.2
  408.2 1.6 copy-start.3
  430.4 1.6 copy-start.2
  431.9 1.6 copy-start.3
  454.1 1.6 copy-start.2
  455.6 1.6 copy-start.3
  477.8 1.6 copy-start.2
  501.4 1.6 copy-start.2
  503.0 1.6 copy-start.3
  527.0 12.8 %copy-start.4 = (f32[2048]{0:T(1024)S(1)}, f32[2048]{0:T(1024)}, u32[]{:S(2)}) copy-start(f32[2048]{0:T(1024)} %param.22) | copy-start | bytes 24580
  527.0 10.5 all-to-all-start
  531.5 396.9 %all-gather.6.cloned.1.call-start = ((), (), s32[]{:S(2)}) async-start(), calls=%async_computation.5 | async-start | bytes 5898240 | tf_op jit(solution)/shard_map/all_gather | solution.py:36
  893.9 72.7 %all-gather.8.cloned.1.call-start = ((), (), s32[]{:S(2)}) async-start(), calls=%async_computation.6 | async-start | bytes 5898240 | tf_op jit(solution)/shard_map/all_gather | solution.py:36
  896.0 154.4 %reduce-scatter.2.cloned.1.call-start = ((), (), s32[]{:S(2)}) async-start(), calls=%async_computation.7 | async-start | bytes 11796480 | tf_op jit(solution)/shard_map/reduce_scatter | solution.py:151
  966.6 5.6 copy-start.5
  966.6 5.6 copy-start.6
  966.6 6.1 copy-start.9
  966.6 9.4 slice-start
  972.6 3.3 slice-start.1
  1080.6 3.3 copy-start.8
  (20 other events, 26.5 us)
Sparse Core Ops, SparseCore 0:
  9.5 54.0 all-gather.3
  894.0 34.3 all-gather.5
  930.1 36.4 all-gather.7
  987.9 62.4 reduce-scatter.1
where the time goes:
time: 1100 us; the launch traced here: 1090 us
  blocking collectives  373 us (34%)
  other arithmetic  250 us (23%)
  waiting for transfers between devices  184 us (17%)
  local copies, waits for them, and re-layouts  142 us (13%)
  matrix products  126 us (11%)
  between operations  13.3 us (1%)
    all_to_all x1, blocking collectives, shards(): lax.all_to_all(outgoing, 'sp', split_axis=0, concat_axis=0, tiled=True)  346 us
    another operation x38, other arithmetic  175 us
    dot_general x18, matrix products, span_terms(): jnp.einsum('qhd,khd->qhk', query_heads, key_rows.reshape(SPAN, local_head...  69.6 us
    convert_element_type x18, other arithmetic, span_terms(): jnp.where(earlier, jnp.exp(jax.nn.log_sigmoid(scores) + later_sum), 0.0)  65.9 us
    all_gather x2, waiting for transfers between devices, on_gathered_pieces(): finished.append(jax.vmap(apply)(lax.all_gather(section, axis), starts))  63 us
    reduce_scatter x1, waiting for transfers between devices, shards(): lax.psum_scatter(lax.optimization_barrier(partial_value.astype(jnp.bfloat...  62.6 us
    cond x108, local copies, waits for them, and re-layouts  53.6 us
    all_gather x1, waiting for transfers between devices, sent_together(): lax.all_gather(both, axis, axis=dim, tiled=True)  52.2 us
  transfers between devices with their start and end apart: 5, of which 5 were waited for; matrix products, arithmetic and copies ran while one was open for 1% of the time, Pallas kernels for 0%

commit v1 on v0

v1 whole, which is shorter than its diff:
```python
import functools

import jax
import jax.numpy as jnp
from jax import lax
from jax.experimental import pallas as pl
from jax.experimental.pallas import tpu as pltpu
from jax.sharding import PartitionSpec as P

HEAD_DIM = 64
TOP = 2
LOG2E = 1.4426950408889634
KEY_CHUNK = 256
ROW_TILE = 512
CHUNKS_PER_STEP = 4


epsilon = 1e-06


def joined_along(blocks, dim):
    blocks = jnp.moveaxis(blocks, 0, dim)
    shape = blocks.shape
    return blocks.reshape(*shape[:dim], shape[dim] * shape[dim + 1], *shape[dim + 2 :])


def on_gathered_pieces(array, axis, dim, apply, out_dim):
    size, width = (lax.axis_size(axis), array.shape[dim])
    count = 2 if width % 2 == 0 else 1
    finished, length = ([], width // count)
    for k in range(count):
        section = lax.slice_in_dim(array, k * length, (k + 1) * length, axis=dim)
        starts = jnp.arange(size) * width + k * length
        finished.append(jax.vmap(apply)(lax.all_gather(section, axis), starts))
    return joined_along(jnp.concatenate(finished, axis=out_dim + 1), out_dim)


def stick_chunk(q, kv, bias2, suffix, later, earlier):
    scores = lax.dot_general(q, kv, (((1,), (1,)), ((), ())), preferred_element_type=jnp.float32)
    z = scores * (HEAD_DIM**-0.5 * LOG2E) + bias2
    softplus = jnp.maximum(jnp.log(1.0 + jnp.exp2(jnp.minimum(z, 126.0))) * LOG2E, z)
    if earlier is not None:
        softplus = jnp.where(earlier, softplus, 0.0)
    after = jnp.dot(softplus.astype(jnp.bfloat16), suffix, preferred_element_type=jnp.float32)
    weights = jnp.exp2(z - softplus - after - jnp.concatenate([later, later], axis=1))
    if earlier is not None:
        weights = jnp.where(earlier, weights, 0.0)
    out = jnp.dot(weights.astype(jnp.bfloat16), kv, preferred_element_type=jnp.float32)
    return out, jnp.sum(softplus, axis=1, keepdims=True)


def attention_kernel(q_ref, kv_ref, bias_ref, suffix_ref, out_ref, total, later):
    me = lax.axis_index("sp")
    rows = q_ref.shape[0]
    own = rows // KEY_CHUNK
    total[...] = jnp.zeros_like(total)
    later[...] = jnp.zeros_like(later)

    def run(c, diagonal):
        kv = kv_ref[pl.ds(pl.multiple_of(c * KEY_CHUNK, KEY_CHUNK), KEY_CHUNK), :]
        bias2 = bias_ref[c]
        for first in range(0, rows, ROW_TILE):
            tile = pl.ds(first, ROW_TILE)
            earlier = None
            if diagonal:
                q_pos = me * rows + first + lax.broadcasted_iota(jnp.int32, (ROW_TILE, KEY_CHUNK), 0)
                k_pos = c * KEY_CHUNK + lax.broadcasted_iota(jnp.int32, (ROW_TILE, KEY_CHUNK), 1)
                earlier = k_pos < q_pos
            out, sums = stick_chunk(q_ref[tile, :], kv, bias2, suffix_ref[...], later[tile, :], earlier)
            total[tile, :] += out
            later[tile, :] += jnp.broadcast_to(sums, (ROW_TILE, 128))

    @pl.loop(0, own)
    def _(j):
        run(me * own + own - 1 - j, True)

    @pl.loop(0, me * own // CHUNKS_PER_STEP)
    def _(j):
        for u in range(CHUNKS_PER_STEP):
            run(me * own - 1 - j * CHUNKS_PER_STEP - u, False)

    out_ref[...] = total[...].astype(out_ref.dtype)


def attention(q, kv, bias2, suffix):
    rows = q.shape[0]
    return pl.pallas_call(
        attention_kernel,
        out_shape=jax.ShapeDtypeStruct((rows, 128), jnp.bfloat16),
        in_specs=[pl.BlockSpec(memory_space=pltpu.VMEM)] * 4,
        out_specs=pl.BlockSpec(memory_space=pltpu.VMEM),
        scratch_shapes=[pltpu.VMEM((rows, 128), jnp.float32), pltpu.VMEM((rows, 128), jnp.float32)],
        compiler_params=pltpu.CompilerParams(vmem_limit_bytes=40 << 20),
        cost_estimate=pl.CostEstimate(flops=20_000_000_000, bytes_accessed=5_000_000, transcendentals=0),
        name="attention",
    )(q, kv, bias2, suffix)


def shards(
    queries,
    keys,
    values,
    key_bias,
    residual,
    out_weight,
    norm_gain,
    routes,
    route_weights,
    gate_weight,
    up_weight,
    down_weight,
):
    sp_count = lax.axis_size("sp")
    kv = lax.all_gather(jnp.concatenate([keys, values], axis=1), "sp", axis=0, tiled=True)
    bias = lax.all_gather(key_bias.reshape(1, -1), "sp", axis=0, tiled=True)
    bias2 = (bias.astype(jnp.float32) * LOG2E).reshape(-1, 1, KEY_CHUNK)
    order = lax.iota(jnp.int32, KEY_CHUNK)
    suffix = (order[:, None] > order[None, :]).astype(jnp.bfloat16)
    attended = attention(jnp.pad(queries, ((0, 0), (0, 128 - HEAD_DIM))), kv, bias2, suffix)[:, HEAD_DIM:]
    token_heads = lax.all_to_all(attended, "tp", split_axis=0, concat_axis=1, tiled=True)
    projected = jnp.dot(token_heads, out_weight, preferred_element_type=jnp.float32)
    stream = (residual.astype(jnp.float32) + projected).astype(jnp.bfloat16).astype(jnp.float32)
    normed = (
        stream * lax.rsqrt(jnp.mean(stream * stream, axis=-1, keepdims=True) + epsilon) * norm_gain
    ).astype(jnp.bfloat16)
    token_count = residual.shape[0]
    width_model = residual.shape[1]
    capacity = max(2, 5 * token_count * TOP // (4 * sp_count))
    flat_routes = routes.reshape(-1)
    onehot = (flat_routes[:, None] == lax.iota(jnp.int32, sp_count)[None, :]).astype(jnp.int32)
    before = jnp.cumsum(onehot, axis=0) - onehot
    slot_of = flat_routes * capacity + jnp.sum(before * onehot, axis=1)
    select = (slot_of[:, None] == lax.iota(jnp.int32, sp_count * capacity)[None, :]).astype(
        jnp.bfloat16
    )
    placing = jnp.sum(select.reshape(token_count, TOP, sp_count * capacity), axis=1)
    outgoing = jnp.einsum("ts,td->sd", placing, normed, preferred_element_type=jnp.float32).astype(
        jnp.bfloat16
    )
    arrived = lax.all_to_all(outgoing, "sp", split_axis=0, concat_axis=0, tiled=True)

    def fan_hidden(row_block, first_row):
        gate_act = jnp.dot(row_block, gate_weight[0], preferred_element_type=jnp.float32)
        up_act = jnp.dot(row_block, up_weight[0], preferred_element_type=jnp.float32)
        return (jax.nn.silu(gate_act) * up_act).astype(jnp.bfloat16)

    hidden = on_gathered_pieces(arrived, "tp", 0, fan_hidden, 0)
    partial_value = jnp.dot(hidden, down_weight[0], preferred_element_type=jnp.float32)
    summed = lax.psum_scatter(
        lax.optimization_barrier(partial_value.astype(jnp.bfloat16))
        .astype(jnp.float32)
        .astype(jnp.bfloat16),
        "tp",
        scatter_dimension=0,
        tiled=True,
    )
    returned = lax.all_to_all(summed, "sp", split_axis=0, concat_axis=0, tiled=True)
    picked = jnp.dot(select, returned, preferred_element_type=jnp.float32).reshape(
        token_count, TOP, width_model
    )
    routed = jnp.sum(picked * route_weights[:, :, None], axis=1)
    return (stream + routed).astype(jnp.bfloat16)


def solution(mesh):
    return jax.shard_map(
        shards,
        mesh=mesh,
        in_specs=(
            P("sp", "tp"),
            P("sp", "tp"),
            P("sp", "tp"),
            P("sp", "tp"),
            P(("sp", "tp"), None),
            P(),
            P(),
            P(("sp", "tp"), None),
            P(("sp", "tp"), None),
            P("sp", None, "tp"),
            P("sp", None, "tp"),
            P("sp", "tp", None),
        ),
        out_specs=P(("sp", "tp"), None),
        check_vma=False,
    )
```

time: 1100 us -> 365 us (0.33)
  blocking collectives: 373 us -> 95.2 us
  other arithmetic: 250 us -> 2.83 us
  local copies, waits for them, and re-layouts: 142 us -> 23.6 us
  matrix products: 126 us -> 34 us
  Pallas kernels: 0 us -> 27.8 us
  waiting for transfers between devices: 184 us -> 158 us
    all_to_all x1, blocking collectives: 346 us -> 45.4 us  [shards(): lax.all_to_all(outgoing, 'sp', split_axis=0, concat_axis=0, tiled=True)]
    another operation x39 -> x2, other arithmetic: 175 us -> 0.63 us
    dot_general x36 -> x0, matrix products: 91.7 us -> none  [the longest x18 69.6 us: span_terms(): jnp.einsum('qhd,khd->qhk', query_heads, key_rows.reshape(SPAN, local_head...]
    convert_element_type x18 -> x1, other arithmetic: 65.9 us -> 0.02 us  [shards(): suffix = (order[:, None] > order[None, :]).astype(jnp.bfloat16)]
    cond x108 -> x0, local copies, waits for them, and re-layouts: 53.6 us -> none
    pallas_call x0 -> x1, Pallas kernels: none -> 27.8 us  [attention(): pl.pallas_call(attention_kernel, out_shape=jax.ShapeDtypeStruct((rows, 12...]
    another operation x74 -> x1, local copies, waits for them, and re-layouts: 26.6 us -> 0.01 us
    all_gather x1, waiting for transfers between devices: 52.2 us -> 26.9 us  [shards(): lax.all_gather(jnp.concatenate([keys, values], axis=1), 'sp', axis=0, til...]
  transfers between devices with their start and end apart: 5 -> 5, of which waited for: 5 -> 5; matrix products, arithmetic and copies ran while one was open for 1% -> 3% of each run, Pallas kernels for 0% -> 0%
where the time goes in v1:
time: 365 us; the launch traced here: 360 us
  waiting for transfers between devices  158 us (43%)
  blocking collectives  95.2 us (26%)
  matrix products  34 us (9%)
  Pallas kernels  27.8 us (8%)
  local copies, waits for them, and re-layouts  23.6 us (6%)
  between operations  13.4 us (4%)
  starting transfers between devices  4.59 us (1%)
    all_gather x2, waiting for transfers between devices, on_gathered_pieces(): finished.append(jax.vmap(apply)(lax.all_gather(section, axis), starts))  62.8 us
    reduce_scatter x1, waiting for transfers between devices, shards(): lax.psum_scatter(lax.optimization_barrier(partial_value.astype(jnp.bfloat...  62.6 us
    all_to_all x1, blocking collectives, shards(): lax.all_to_all(outgoing, 'sp', split_axis=0, concat_axis=0, tiled=True)  45.4 us
    pallas_call x1, Pallas kernels, attention(): pl.pallas_call(attention_kernel, out_shape=jax.ShapeDtypeStruct((rows, 12...  27.8 us
    all_to_all x1, blocking collectives, shards(): lax.all_to_all(summed, 'sp', split_axis=0, concat_axis=0, tiled=True)  27.1 us
    all_gather x1, waiting for transfers between devices, shards(): lax.all_gather(jnp.concatenate([keys, values], axis=1), 'sp', axis=0, til...  26.9 us
    all_gather x1, blocking collectives, shards(): bias = lax.all_gather(key_bias.reshape(1, -1), 'sp', axis=0, tiled=True)  22.7 us
    dot_general x2, matrix products, fan_hidden(): jnp.dot(row_block, up_weight[0], preferred_element_type=jnp.float32)  13.2 us
  transfers between devices with their start and end apart: 5, of which 5 were waited for; matrix products, arithmetic and copies ran while one was open for 3% of the time, Pallas kernels for 0%

profile of v1, /device:TPU:64, one launch (start us, length us, event | category | flops | bytes accessed | tf_op | source)
XLA Modules:
  0.0 359.9 jit_solution(4823542928451561223)
XLA Ops:
  6.5 1.2 copy.49
  7.8 1.1 copy.50
  8.9 0.9 pad_maximum_fusion.1
  9.7 0.0 all-gather.5.cloned.1.call-update
  9.8 0.8 copy.52
  10.5 0.1 eq.65
  10.7 0.1 eq.61
  10.8 0.6 reduce-window.6
  11.4 0.2 slice_reduce_fusion
  11.7 0.1 fusion.26
  11.7 0.1 reduce_sum.42
  11.9 0.1 copy.55
  12.0 1.1 copy.48
  13.1 0.1 pad.4.q_ref
  13.1 22.7 %all-gather = bf16[16384,1]{0,1:T(2,128)(2,1)S(1)} all-gather(bf16[1024,1]{0,1:T(2,128)(2,1)S(1)} %copy-done.4), channel_id=2, replica_groups=mesh['sp'=16,'tp'=8] {'sp'}, dimensions={0}, use_global_device_ids=true | all-gather | bytes 34816 | tf_op jit(solution)/shard_map/all_gather | solution.py:115
  35.9 0.1 convert_multiply_fusion
  36.0 26.9 %all-gather.5.cloned.1.call-done.kv_ref = bf16[16384,128]{1,0:T(8,128)(2,1)} async-done(((bf16[1024,128]{1,0:T(8,128)(2,1)}), bf16[16384,128]{1,0:T(8,128)(2,1)}) %all-gather.5.cloned.1.call-update) | async-done | bytes 4194320 | tf_op jit(solution)/shard_map/all_gather | solution.py:114
  62.9 2.2 copy-done.1
  65.1 27.8 %attention.1 = bf16[1024,128]{1,0:T(8,128)(2,1)S(1)} custom-call(bf16[1024,128]{1,0:T(8,128)(2,1)S(1)} %pad.4.q_ref, bf16[16384,128]{1,0:T(8,128)(2,1)S(1)} %copy-done.1, f32[64,1,256]{2,1,0:T(1,128)S(1)} %bitcast.56, bf16[256,256]{1,0:T(8,128)(2,1)S(1)} %fusion.21.suffix_ref), custom_call_target="tpu_custom_call" | custom-call | flops 20000000000 | bytes 5000000 | tf_op jit(solution)/shard_map/attention/pallas_call | solution.py:87
  92.9 0.1 slice.22
  93.1 0.8 copy.51
  93.9 4.3 %all-to-all-start = ((bf16[8,128,64]{1,2,0:T(8,128)(2,1)}), bf16[8,128,64]{1,2,0:T(8,128)(2,1)S(1)}, u32[]{:S(2)}, u32[]{:S(2)}) async-start(bf16[8,128,64]{1,2,0:T(8,128)(2,1)} %copy.51), calls=%async_computation | async-start | bytes 262144 | tf_op jit(solution)/shard_map/all_to_all | solution.py:120
  98.2 0.0 all-gather.7.cloned.1.call-start
  98.2 6.0 %all-to-all-done = bf16[8,128,64]{1,2,0:T(8,128)(2,1)S(1)} async-done(((bf16[8,128,64]{1,2,0:T(8,128)(2,1)}), bf16[8,128,64]{1,2,0:T(8,128)(2,1)S(1)}, u32[]{:S(2)}, u32[]{:S(2)}) %all-to-all-start) | async-done | bytes 131104 | tf_op jit(solution)/shard_map/all_to_all | solution.py:120
  104.3 2.2 multiply_reduce_fusion
  106.5 1.6 convolution_convert_fusion.1
  108.1 3.2 all_to_all.32
  111.3 45.4 %all_to_all.40 = bf16[16,20,2048]{2,1,0:T(8,128)(2,1)S(1)} all-to-all(bf16[16,20,2048]{2,1,0:T(8,128)(2,1)} %all_to_all.32), channel_id=1, replica_groups=mesh['sp'=16,'tp'=8] {'sp'}, dimensions={0} | all-to-all | bytes 2621440 | tf_op jit(solution)/shard_map/all_to_all | solution.py:140
  156.8 1.4 fusion.28
  158.1 2.0 all_gather.20
  160.2 0.0 all-gather.9.cloned.1.call-start
  160.2 2.1 all_gather.22
  162.3 0.2 reduce-scatter.2.cloned.1.call-start
  162.6 32.2 %all-gather.7.cloned.1.call-done = bf16[8,160,2048]{2,1,0:T(8,128)(2,1)} async-done(((bf16[1,160,2048]{2,1,0:T(8,128)(2,1)}), bf16[8,160,2048]{2,1,0:T(8,128)(2,1)}) %all-gather.7.cloned.1.call-update) | async-done | bytes 5242896 | tf_op jit(solution)/shard_map/all_gather | solution.py:34
  194.7 7.6 %fusion.5 = f32[8,160,512]{2,1,0:T(8,128)} fusion(bf16[8,160,2048]{2,1,0:T(8,128)(2,1)} %all-gather.7.cloned.1.call-done, bf16[1,2048,512]{2,1,0:T(8,128)(2,1)} %param.22), kind=kOutput, calls=%fused_computation.12 | convolution fusion | flops 2684354560 | bytes 9961472 | tf_op jit(solution)/shard_map/vmap()/dot_general | solution.py:144
  202.3 30.6 %all-gather.9.cloned.1.call-done = bf16[8,160,2048]{2,1,0:T(8,128)(2,1)} async-done(((bf16[1,160,2048]{2,1,0:T(8,128)(2,1)}), bf16[8,160,2048]{2,1,0:T(8,128)(2,1)}) %all-gather.9.cloned.1.call-update) | async-done | bytes 5242896 | tf_op jit(solution)/shard_map/all_gather | solution.py:34
  232.9 5.6 %fusion.3 = f32[8,160,512]{2,1,0:T(8,128)S(1)} fusion(bf16[8,160,2048]{2,1,0:T(8,128)(2,1)} %all-gather.9.cloned.1.call-done, bf16[1,2048,512]{2,1,0:T(8,128)(2,1)} %param.22), kind=kOutput, calls=%fused_computation.10 | convolution fusion | flops 2684354560 | bytes 9961472 | tf_op jit(solution)/shard_map/vmap()/dot_general | solution.py:144
  238.5 0.4 copy-done.8
  239.0 3.3 multiply_convert_fusion.1
  242.3 3.3 multiply_convert_fusion
  245.7 0.2 pad_maximum_fusion
  245.8 8.2 %convolution_convert_fusion = bf16[2560,2048]{1,0:T(8,128)(2,1)} fusion(bf16[2560,512]{1,0:T(8,128)(2,1)S(1)} %bitcast.57, bf16[1,512,2048]{2,1,0:T(8,128)(2,1)S(1)} %copy-done), kind=kOutput, calls=%fused_computation | convolution fusion | flops 5373952000 | bytes 15204352 | tf_op jit(solution)/shard_map/dot_general | solution.py:148
  254.1 62.6 %reduce-scatter.2.cloned.1.call-done = bf16[320,2048]{1,0:T(8,128)(2,1)} async-done(((bf16[2560,2048]{1,0:T(8,128)(2,1)}), bf16[320,2048]{1,0:T(8,128)(2,1)}) %reduce-scatter.2.cloned.1.call-update) | async-done | bytes 1310736 | tf_op jit(solution)/shard_map/reduce_scatter | solution.py:149
  316.7 3.2 all_to_all.34
  319.9 27.1 %all_to_all.41 = bf16[16,20,2048]{2,1,0:T(8,128)(2,1)} all-to-all(bf16[16,20,2048]{2,1,0:T(8,128)(2,1)} %all_to_all.34), channel_id=1, replica_groups=mesh['sp'=16,'tp'=8] {'sp'}, dimensions={0} | all-to-all | bytes 2621440 | tf_op jit(solution)/shard_map/all_to_all | solution.py:157
  347.0 3.3 reshape.100
  350.3 2.1 fusion.15
  352.4 0.9 add_convert_fusion
  (32 shorter events, 0.2 us)
Async XLA Ops:
  6.5 239.3 %copy-start = (bf16[1,512,2048]{2,1,0:T(8,128)(2,1)S(1)}, bf16[1,512,2048]{2,1,0:T(8,128)(2,1)}, u32[]{:S(2)}) copy-start(bf16[1,512,2048]{2,1,0:T(8,128)(2,1)} %param.23) | copy-start | bytes 6291460
  6.5 29.3 %copy-start.3 = (s32[128,2]{0,1:T(2,128)S(1)}, s32[128,2]{0,1:T(2,128)}, u32[]{:S(2)}) copy-start(s32[128,2]{0,1:T(2,128)} %param.19) | copy-start | bytes 3076
  6.5 6.6 %copy-start.4 = (bf16[1024,1]{0,1:T(2,128)(2,1)S(1)}, bf16[1024,1]{0,1:T(2,128)(2,1)}, u32[]{:S(2)}) copy-start(bf16[1024,1]{0,1:T(2,128)(2,1)} %param.15) | copy-start | bytes 6148
  6.5 56.4 %all-gather.5.cloned.1.call-start = ((), (), s32[]{:S(2)}) async-start(), calls=%async_computation.4 | async-start | bytes 4456448 | tf_op jit(solution)/shard_map/all_gather | solution.py:114
  62.9 2.2 copy-start.1
  92.9 13.6 %copy-start.2 = (f32[2048]{0:T(1024)S(1)}, f32[2048]{0:T(1024)}, u32[]{:S(2)}) copy-start(f32[2048]{0:T(1024)} %param.18) | copy-start | bytes 24580
  93.9 10.4 %all-to-all-start = ((bf16[8,128,64]{1,2,0:T(8,128)(2,1)}), bf16[8,128,64]{1,2,0:T(8,128)(2,1)S(1)}, u32[]{:S(2)}, u32[]{:S(2)}) async-start(bf16[8,128,64]{1,2,0:T(8,128)(2,1)} %copy.51), calls=%async_computation | async-start | bytes 262144 | tf_op jit(solution)/shard_map/all_to_all | solution.py:120
  98.2 96.6 %all-gather.7.cloned.1.call-start = ((), (), s32[]{:S(2)}) async-start(), calls=%async_computation.5 | async-start | bytes 5898240 | tf_op jit(solution)/shard_map/all_gather | solution.py:34
  160.2 72.7 %all-gather.9.cloned.1.call-start = ((), (), s32[]{:S(2)}) async-start(), calls=%async_computation.6 | async-start | bytes 5898240 | tf_op jit(solution)/shard_map/all_gather | solution.py:34
  162.3 154.4 %reduce-scatter.2.cloned.1.call-start = ((), (), s32[]{:S(2)}) async-start(), calls=%async_computation.7 | async-start | bytes 11796480 | tf_op jit(solution)/shard_map/reduce_scatter | solution.py:149
  232.9 5.6 %copy-start.5 = (bf16[8,160,2048]{2,1,0:T(8,128)(2,1)S(1)}, bf16[8,160,2048]{2,1,0:T(8,128)(2,1)}, u32[]{:S(2)}) copy-start(bf16[8,160,2048]{2,1,0:T(8,128)(2,1)} %all-gather.7.cloned.1.call-done) | copy-start | bytes 15728644
  232.9 5.6 %copy-start.6 = (bf16[1,2048,512]{2,1,0:T(8,128)(2,1)S(1)}, bf16[1,2048,512]{2,1,0:T(8,128)(2,1)}, u32[]{:S(2)}) copy-start(bf16[1,2048,512]{2,1,0:T(8,128)(2,1)} %param.21) | copy-start | bytes 6291460
  232.9 6.1 %copy-start.8 = (f32[8,160,512]{2,1,0:T(8,128)S(1)}, f32[8,160,512]{2,1,0:T(8,128)}, u32[]{:S(2)}) copy-start(f32[8,160,512]{2,1,0:T(8,128)} %fusion.5) | copy-start | bytes 7864324
  232.9 9.4 %slice-start = ((s8[5242880]{0:T(1024)(128)(4,1)}), s8[4194304]{0:T(1024)(128)(4,1)S(1)}, s32[]{:S(2)}) async-start(s8[5242880]{0:T(1024)(128)(4,1)} %bitcast.60), calls=%async_computation.8 | async-start | bytes 8388608
  239.0 3.3 slice-start.1
  319.9 30.4 %copy-start.7 = (f32[128,2]{0,1:T(2,128)S(1)}, f32[128,2]{0,1:T(2,128)}, u32[]{:S(2)}) copy-start(f32[128,2]{0,1:T(2,128)} %param.20) | copy-start | bytes 3076
Sparse Core Ops, SparseCore 0:
  9.9 52.9 all-gather.4
  160.3 34.3 all-gather.6
  196.4 36.4 all-gather.8
  254.2 62.4 reduce-scatter.1
